TPU v7x, 512 devices: a whole 4x4x16 slice. The times are simulated.
512 devices in a mesh: sp: 32 (over z, core), tp: 16 (over y, x).
Axes of the slice: x: 4, y: 4, z: 16, core: 2. Of those that a mesh axis runs over, the one named last changes fastest.
Arguments:
- moe_input: bfloat16 [4096, 2048], P('sp', 'tp'), may hold values from -6 to 6
- cotangent: bfloat16 [4096, 2048], P('sp', 'tp'), may hold values from -6 to 6
- routes: int32 [4096, 2], P('sp'), may hold values from 0 to 31, all different within a row; in each aligned block of 128 rows (0 to 127, 128 to 255, ...) at most 16 rows name the same one
- route_weight: float32 [4096, 2], P('sp'), may hold values from 0.1 to 1
- w_gate: bfloat16 [32, 2816, 2048], P('sp', 'tp'), may hold values from -0.125 to 0.125
- w_up: bfloat16 [32, 2816, 2048], P('sp', 'tp'), may hold values from -0.125 to 0.125
- w_down: bfloat16 [32, 2816, 2048], P('sp', 'tp'), may hold values from -0.109375 to 0.109375
- v_value: bfloat16 [4096, 1024], P('sp', 'tp'), may hold values from -6 to 6
- v_gate: bfloat16 [4096, 1024], P('sp', 'tp'), may hold values from -12 to 12
- conv_out: bfloat16 [4096, 1024], P('sp', 'tp'), may hold values from -6 to 6
- row_mean: float32 [4096], P('sp'), may hold values from -3 to 3
- row_rstd: float32 [4096], P('sp'), may hold values from 0.5 to 2
- ln_gain: float32 [1024], P('tp'), may hold values from 0.1 to 1.9
- taps: bfloat16 [31, 1024], P(None, 'tp'), may hold values from -1 to 1
- out_proj: bfloat16 [2048, 1024], P('sp', 'tp'), may hold values from -0.1875 to 0.1875
Outputs:
- gate_grad: bfloat16 [32, 2816, 2048], P('sp', 'tp')
- up_grad: bfloat16 [32, 2816, 2048], P('sp', 'tp')
- down_grad: bfloat16 [32, 2816, 2048], P('sp', 'tp')
- proj_grad: float32 [2048, 1024], P('sp', 'tp')
- stream_grad: bfloat16 [4096, 2048], P('sp', 'tp')
- value_grad: bfloat16 [4096, 1024], P('sp', 'tp')
- gating_grad: bfloat16 [4096, 1024], P('sp', 'tp')
Inputs may be any that keep to these rules, and one draw needn't show every extreme that they name: `routes`: in the rows of one device no expert is named more than 16 times.
All inputs are finite; a program needn't handle non-finite values.
Results may differ from a plain program's by a relative error of at most 0.025.
Values may be sent and summed in bfloat16 or wider, within the bound.
A program may use at most 64 MiB of HBM per device.

v0:
```python
import jax
import jax.numpy as jnp
from jax import lax
from jax.sharding import PartitionSpec as P


def side_by_side(arrays, axis, split_dim, concat_dim, along):
    ends, at = ([], 0)
    for a in arrays[:-1]:
        at += a.shape[along]
        ends.append(at)
    both = jnp.concatenate(arrays, axis=along)
    return tuple(
        jnp.split(
            lax.all_to_all(both, axis, split_axis=split_dim, concat_axis=concat_dim, tiled=True),
            ends,
            axis=along,
        )
    )


def in_one_piece(arrays, axis, dim, along):
    both = jnp.concatenate(arrays, axis=along)
    result, at, finished = (lax.all_gather(both, axis, axis=dim, tiled=True), 0, [])
    for a in arrays:
        finished.append(lax.slice_in_dim(result, at, at + a.shape[along], axis=along))
        at += a.shape[along]
    return tuple(finished)


def cut_along(value, dim, peers):
    shape = value.shape
    blocks = value.reshape(*shape[:dim], peers, shape[dim] // peers, *shape[dim + 1 :])
    return jnp.moveaxis(blocks, dim, 0)


def summed_on_arrival(value, axis, dim):
    blocks = cut_along(value, dim, lax.axis_size(axis))
    arrived = lax.all_to_all(blocks, axis, split_axis=0, concat_axis=0, tiled=True)
    return arrived.astype(jnp.float32).sum(axis=0)


def from_everyone(value, axis):
    copies = jnp.broadcast_to(value, (lax.axis_size(axis), *value.shape))
    return lax.all_to_all(copies, axis, split_axis=0, concat_axis=0, tiled=True)


def joined_along(blocks, dim):
    blocks = jnp.moveaxis(blocks, 0, dim)
    shape = blocks.shape
    return blocks.reshape(*shape[:dim], shape[dim] * shape[dim + 1], *shape[dim + 2 :])


def collect(value, axis, dim):
    blocks = from_everyone(value, axis)
    return joined_along(blocks, dim)


def of_everyone(value, axis):
    return from_everyone(value, axis).sum(axis=0)


def together(arrays, axis):
    vector, at, finished = (jnp.concatenate([a.reshape(-1) for a in arrays]), 0, [])
    subtotal = of_everyone(vector, axis)
    for a in arrays:
        finished.append(subtotal[at : at + a.size].reshape(a.shape))
        at += a.size
    return tuple(finished)


def passed_along(value, axis, steps):
    count = lax.axis_size(axis)
    leading, last = (max(0, -steps), min(count, count - steps))
    return lax.ppermute(value, axis, [(source, source + steps) for source in range(leading, last)])


def route_targets(routes, experts, capacity):
    flat_routes = routes.reshape(-1)
    member = (flat_routes[:, None] == jnp.arange(experts, dtype=jnp.int32)[None, :]).astype(
        jnp.int32
    )
    earlier = jnp.cumsum(member, axis=0) - member
    slot_index = jnp.sum(earlier * member, axis=1)
    return flat_routes * capacity + slot_index


def contract_rows(left, right):
    return lax.dot_general(
        left, right, (((0,), (0,)), ((), ())), preferred_element_type=jnp.float32
    )


def contract_cols(left, right):
    return lax.dot_general(
        left, right, (((1,), (1,)), ((), ())), preferred_element_type=jnp.float32
    )


def shards(
    moe_input,
    cotangent,
    routes,
    route_weight,
    w_gate,
    w_up,
    w_down,
    v_value,
    v_gate,
    conv_out,
    row_mean,
    row_rstd,
    ln_gain,
    taps,
    out_proj,
):
    experts = lax.axis_size("sp")
    tokens = routes.shape[0]
    capacity = 4 * tokens // experts
    total = experts * capacity
    buffer_row = route_targets(routes, experts, capacity)
    token_index = jnp.arange(2 * tokens, dtype=jnp.int32) // 2
    weights = route_weight.reshape(-1)
    width = moe_input.shape[1]
    picked = moe_input[token_index]
    weighted = (weights[:, None] * cotangent[token_index].astype(jnp.float32)).astype(jnp.bfloat16)
    rows_buf = jnp.zeros((total, width), jnp.bfloat16).at[buffer_row].set(picked)
    cotan_buf = jnp.zeros((total, width), jnp.bfloat16).at[buffer_row].set(weighted)
    rows_buf, cotan_buf = (
        rows_buf.reshape(experts, capacity, width),
        cotan_buf.reshape(experts, capacity, width),
    )
    part_rows, part_cotan = side_by_side((rows_buf, cotan_buf), "sp", 0, 0, 1)
    arrived_rows, arrived_cotan = in_one_piece((part_rows, part_cotan), "tp", 2, 0)
    width = arrived_rows.shape[2]
    expert_in = arrived_rows.reshape(total, width)
    expert_cot = arrived_cotan.reshape(total, width)
    gate_w = w_gate[0]
    up_w = w_up[0]
    down_w = w_down[0]
    gate_pre = contract_cols(expert_in, gate_w)
    up_pre = contract_cols(expert_in, up_w)
    gate_sig = jax.nn.sigmoid(gate_pre)
    gate_act = gate_pre * gate_sig
    hidden = (gate_act * up_pre).astype(jnp.bfloat16)
    down_g = contract_rows(hidden, expert_cot).astype(jnp.bfloat16)
    hidden_grad = contract_cols(expert_cot, down_w)
    gate_delta = (hidden_grad * up_pre * gate_sig * (1.0 + gate_pre * (1.0 - gate_sig))).astype(
        jnp.bfloat16
    )
    up_delta = (hidden_grad * gate_act).astype(jnp.bfloat16)
    gate_g = contract_rows(gate_delta, expert_in).astype(jnp.bfloat16)
    up_g = contract_rows(up_delta, expert_in).astype(jnp.bfloat16)
    partial_value = jnp.dot(gate_delta, gate_w, preferred_element_type=jnp.float32) + jnp.dot(
        up_delta, up_w, preferred_element_type=jnp.float32
    )
    row_share = summed_on_arrival(partial_value.astype(jnp.bfloat16), "tp", 1).astype(jnp.bfloat16)
    slice_width = row_share.shape[1]
    returned = lax.all_to_all(
        row_share.reshape(experts, capacity, slice_width),
        "sp",
        split_axis=0,
        concat_axis=0,
        tiled=True,
    )
    mine = (
        returned.reshape(total, slice_width)[buffer_row]
        .astype(jnp.float32)
        .reshape(tokens, 2, slice_width)
    )
    stream = (cotangent.astype(jnp.float32) + (mine[:, 0] + mine[:, 1])).astype(jnp.bfloat16)
    full_stream = collect(stream, "tp", 1)
    normed = (conv_out.astype(jnp.float32) - row_mean[:, None]) * row_rstd[:, None]
    scaled_norm = normed * ln_gain[None, :]
    norm_sig = jax.nn.sigmoid(scaled_norm)
    mixed = (scaled_norm * norm_sig).astype(jnp.bfloat16)
    columns = full_stream
    mixed_grad = jnp.dot(
        columns,
        lax.all_gather(out_proj, "sp", axis=0, tiled=True),
        preferred_element_type=jnp.float32,
    )
    columns = full_stream
    proj_g = summed_on_arrival(contract_rows(columns, mixed).astype(jnp.bfloat16), "sp", 0)
    channels = out_proj.shape[1] * lax.axis_size("tp")
    norm_grad = mixed_grad * norm_sig * (1.0 + scaled_norm * (1.0 - norm_sig)) * ln_gain[None, :]
    first_sum, second_sum = together(
        (jnp.sum(norm_grad, axis=1), jnp.sum(norm_grad * normed, axis=1)), "tp"
    )
    first_mean = first_sum[:, None] / channels
    second_mean = second_sum[:, None] / channels
    conv_grad = row_rstd[:, None] * (norm_grad - first_mean - normed * second_mean)
    kernel = taps.shape[0]
    following = passed_along(conv_grad[: kernel - 1], "sp", -1)
    extended = jnp.concatenate([conv_grad, following], axis=0)
    tap_values = taps.astype(jnp.float32)
    unit_grad = jnp.zeros_like(conv_grad)
    for offset in range(kernel):
        lead = kernel - 1 - offset
        unit_grad = unit_grad + tap_values[offset][None, :] * extended[lead : lead + tokens]
    value_sig = jax.nn.sigmoid(v_gate.astype(jnp.float32))
    value_g = (unit_grad * value_sig).astype(jnp.bfloat16)
    gating_g = (unit_grad * v_value.astype(jnp.float32) * value_sig * (1.0 - value_sig)).astype(
        jnp.bfloat16
    )
    return (gate_g[None], up_g[None], down_g[None], proj_g, stream, value_g, gating_g)


def solution(mesh):
    return jax.shard_map(
        shards,
        mesh=mesh,
        in_specs=(
            P("sp", "tp"),
            P("sp", "tp"),
            P("sp", None),
            P("sp", None),
            P("sp", "tp", None),
            P("sp", "tp", None),
            P("sp", "tp", None),
            P("sp", "tp"),
            P("sp", "tp"),
            P("sp", "tp"),
            P("sp"),
            P("sp"),
            P("tp"),
            P(None, "tp"),
            P("sp", "tp"),
        ),
        out_specs=(
            P("sp", "tp", None),
            P("sp", "tp", None),
            P("sp", "tp", None),
            P("sp", "tp"),
            P("sp", "tp"),
            P("sp", "tp"),
            P("sp", "tp"),
        ),
        check_vma=False,
    )
```

profile of v0, /device:TPU:1, one launch (start us, length us, event | category | flops | bytes accessed | tf_op | source)
XLA Modules:
  0.0 267.1 jit_solution(11053824604660683432)
XLA Ops:
  11.2 3.1 %scatter_custom_fusion = bf16[512,128]{1,0:T(8,128)(2,1)S(1)} fusion(s32[256]{0:T(256)S(1)} %bitcast.168, bf16[128,128]{1,0:T(8,128)(2,1)} %param.15, s32[1024]{0:T(1024)S(1)} %pad_clamp_fusion.1, bf16[]{:T(256)} %constant.30.clone.1), kind=kCustom, calls=%fused_computation.97 | custom fusion | bytes 131584 | tf_op jit(solution)/shard_map/scatter | solution.py:127
  14.3 3.2 %scatter_custom_fusion.1 = bf16[512,128]{1,0:T(8,128)(2,1)S(1)} fusion(s32[256]{0:T(256)S(1)} %bitcast.169, f32[256]{0:T(256)S(1)} %mul.427, bf16[]{:T(256)} %constant.30.clone.1, bf16[128,128]{1,0:T(8,128)(2,1)} %param.16, s32[1024]{0:T(1024)S(1)} %pad_clamp_fusion.1), kind=kCustom, calls=%fused_computation.94 | custom fusion | flops 98304 | bytes 168962 | tf_op jit(solution)/shard_map/scatter | solution.py:128
  17.6 38.8 %all_to_all.31 = bf16[32,32,128]{2,1,0:T(8,128)(2,1)S(1)} all-to-all(bf16[32,32,128]{2,1,0:T(8,128)(2,1)S(1)} %pad_maximum_fusion), channel_id=1, replica_groups=mesh['sp'=32,'tp'=16] {'sp'}, dimensions={0} | all-to-all | bytes 524288 | tf_op jit(solution)/shard_map/all_to_all | solution.py:15
  57.1 62.2 %all-gather.2.cloned.1.call-done = bf16[64,16,2048]{2,1,0:T(8,128)(2,1)} async-done(((bf16[64,16,128]{2,1,0:T(8,128)(2,1)}), bf16[64,16,2048]{2,1,0:T(8,128)(2,1)}) %all-gather.2.cloned.1.call-update) | async-done | bytes 4194320 | tf_op jit(solution)/shard_map/all_gather | solution.py:24
  119.4 2.6 fusion.127
  127.4 1.9 copy.80
  129.3 4.8 %all-to-all-start.1 = ((bf16[16,512,128]{2,1,0:T(8,128)(2,1)}), bf16[16,512,128]{2,1,0:T(8,128)(2,1)}, u32[]{:S(2)}, u32[]{:S(2)}) async-start(bf16[16,512,128]{2,1,0:T(8,128)(2,1)} %bitcast.155), calls=%async_computation.1 | async-start | bytes 4194304 | tf_op jit(solution)/shard_map/all_to_all | solution.py:39
  134.2 37.3 %all_gather.7 = bf16[2048,64]{1,0:T(8,128)(2,1)} all-gather(bf16[64,64]{1,0:T(8,128)(2,1)S(1)} %copy-done.9), channel_id=1, replica_groups=mesh['sp'=32,'tp'=16] {'sp'}, dimensions={0}, use_global_device_ids=true | all-gather | bytes 270336 | tf_op jit(solution)/shard_map/all_gather | solution.py:180
  171.5 2.6 reduce_sum.61
  174.0 8.9 %all-to-all-start.2 = ((bf16[32,16,128]{2,1,0:T(8,128)(2,1)}), bf16[32,16,128]{2,1,0:T(8,128)(2,1)S(1)}, u32[]{:S(2)}, u32[]{:S(2)}) async-start(bf16[32,16,128]{2,1,0:T(8,128)(2,1)} %bitcast.15), calls=%async_computation.2 | async-start | bytes 262144 | tf_op jit(solution)/shard_map/all_to_all | solution.py:159
  184.2 14.5 %all-to-all-done.2 = bf16[32,16,128]{2,1,0:T(8,128)(2,1)S(1)} async-done(((bf16[32,16,128]{2,1,0:T(8,128)(2,1)}), bf16[32,16,128]{2,1,0:T(8,128)(2,1)S(1)}, u32[]{:S(2)}, u32[]{:S(2)}) %all-to-all-start.2) | async-done | bytes 131104 | tf_op jit(solution)/shard_map/all_to_all | solution.py:159
  200.8 6.9 %all-to-all-start.3 = ((bf16[16,128,128]{1,2,0:T(8,128)(2,1)}), bf16[16,128,128]{1,2,0:T(8,128)(2,1)S(1)}, u32[]{:S(2)}, u32[]{:S(2)}) async-start(bf16[16,128,128]{1,2,0:T(8,128)(2,1)} %broadcast_in_dim.13), calls=%async_computation.3 | async-start | bytes 1048576 | tf_op jit(solution)/shard_map/all_to_all | solution.py:45
  207.7 2.5 fusion
  211.7 6.0 %all-to-all-done.3 = bf16[16,128,128]{1,2,0:T(8,128)(2,1)S(1)} async-done(((bf16[16,128,128]{1,2,0:T(8,128)(2,1)}), bf16[16,128,128]{1,2,0:T(8,128)(2,1)S(1)}, u32[]{:S(2)}, u32[]{:S(2)}) %all-to-all-start.3) | async-done | bytes 524320 | tf_op jit(solution)/shard_map/all_to_all | solution.py:45
  217.7 2.0 fusion.125
  220.3 3.5 %all-to-all-start.5 = ((f32[16,1,256]{2,1,0:T(1,128)}), f32[16,1,256]{2,1,0:T(1,128)S(1)}, u32[]{:S(2)}, u32[]{:S(2)}) async-start(f32[16,1,256]{2,1,0:T(1,128)} %broadcast_in_dim.14), calls=%async_computation.5 | async-start | bytes 32768 | tf_op jit(solution)/shard_map/all_to_all | solution.py:45
  223.8 1.8 convolution_convert_fusion.3
  225.6 1.5 reshape.156
  228.4 2.1 reshape.215
  230.5 6.9 %all-to-all-start.4 = ((bf16[32,2,2048]{2,1,0:T(2,128)(2,1)}), bf16[32,2,2048]{2,1,0:T(2,128)(2,1)S(1)}, u32[]{:S(2)}, u32[]{:S(2)}) async-start(bf16[32,2,2048]{2,1,0:T(2,128)(2,1)} %reshape.215), calls=%async_computation.4 | async-start | bytes 524288 | tf_op jit(solution)/shard_map/all_to_all | solution.py:39
  238.3 2.3 collective-permute-start
  241.9 8.5 %collective-permute-done = f32[30,64]{0,1:T(8,128)S(1)} collective-permute-done((f32[30,64]{0,1:T(8,128)S(1)}, f32[30,64]{0,1:T(8,128)S(1)}, u32[]{:S(2)}, u32[]{:S(2)}) %collective-permute-start) | collective-permute-done | bytes 7712 | tf_op jit(solution)/shard_map/ppermute | solution.py:75
  250.8 1.5 multiply_convert_fusion.6
  252.9 6.1 %all-to-all-done.4 = bf16[32,2,2048]{2,1,0:T(2,128)(2,1)S(1)} async-done(((bf16[32,2,2048]{2,1,0:T(2,128)(2,1)}), bf16[32,2,2048]{2,1,0:T(2,128)(2,1)S(1)}, u32[]{:S(2)}, u32[]{:S(2)}) %all-to-all-start.4) | async-done | bytes 262176 | tf_op jit(solution)/shard_map/all_to_all | solution.py:39
  (146 shorter events, 20.6 us)
Async XLA Ops:
  7.2 114.9 %copy-start = (bf16[1,176,2048]{2,1,0:T(8,128)(2,1)S(1)}, bf16[1,176,2048]{2,1,0:T(8,128)(2,1)}, u32[]{:S(2)}) copy-start(bf16[1,176,2048]{2,1,0:T(8,128)(2,1)} %param.19) | copy-start | bytes 2162692
  7.2 112.2 %all-gather.2.cloned.1.call-start = ((), (), s32[]{:S(2)}) async-start(), calls=%async_computation.6 | async-start | bytes 4456448 | tf_op jit(solution)/shard_map/all_gather | solution.py:24
  129.3 42.2 %all-to-all-start.1 = ((bf16[16,512,128]{2,1,0:T(8,128)(2,1)}), bf16[16,512,128]{2,1,0:T(8,128)(2,1)}, u32[]{:S(2)}, u32[]{:S(2)}) async-start(bf16[16,512,128]{2,1,0:T(8,128)(2,1)} %bitcast.155), calls=%async_computation.1 | async-start | bytes 4194304 | tf_op jit(solution)/shard_map/all_to_all | solution.py:39
  134.2 65.6 %copy-start.6 = (bf16[128,128]{1,0:T(8,128)(2,1)S(1)}, bf16[128,128]{1,0:T(8,128)(2,1)}, u32[]{:S(2)}) copy-start(bf16[128,128]{1,0:T(8,128)(2,1)} %param.16) | copy-start | bytes 98308
  174.0 24.7 %all-to-all-start.2 = ((bf16[32,16,128]{2,1,0:T(8,128)(2,1)}), bf16[32,16,128]{2,1,0:T(8,128)(2,1)S(1)}, u32[]{:S(2)}, u32[]{:S(2)}) async-start(bf16[32,16,128]{2,1,0:T(8,128)(2,1)} %bitcast.15), calls=%async_computation.2 | async-start | bytes 262144 | tf_op jit(solution)/shard_map/all_to_all | solution.py:159
  200.8 16.9 %all-to-all-start.3 = ((bf16[16,128,128]{1,2,0:T(8,128)(2,1)}), bf16[16,128,128]{1,2,0:T(8,128)(2,1)S(1)}, u32[]{:S(2)}, u32[]{:S(2)}) async-start(bf16[16,128,128]{1,2,0:T(8,128)(2,1)} %broadcast_in_dim.13), calls=%async_computation.3 | async-start | bytes 1048576 | tf_op jit(solution)/shard_map/all_to_all | solution.py:45
  220.3 10.2 %all-to-all-start.5 = ((f32[16,1,256]{2,1,0:T(1,128)}), f32[16,1,256]{2,1,0:T(1,128)S(1)}, u32[]{:S(2)}, u32[]{:S(2)}) async-start(f32[16,1,256]{2,1,0:T(1,128)} %broadcast_in_dim.14), calls=%async_computation.5 | async-start | bytes 32768 | tf_op jit(solution)/shard_map/all_to_all | solution.py:45
  228.1 22.4 %copy-start.14 = (f32[64]{0:T(128)S(1)}, f32[64]{0:T(128)}, u32[]{:S(2)}) copy-start(f32[64]{0:T(128)} %get-tuple-element.61) | copy-start | bytes 772
  228.1 22.4 %copy-start.15 = (f32[64]{0:T(128)S(1)}, f32[64]{0:T(128)}, u32[]{:S(2)}) copy-start(f32[64]{0:T(128)} %get-tuple-element.62) | copy-start | bytes 772
  228.1 22.4 %copy-start.16 = (f32[64]{0:T(128)S(1)}, f32[64]{0:T(128)}, u32[]{:S(2)}) copy-start(f32[64]{0:T(128)} %get-tuple-element.63) | copy-start | bytes 772
  228.1 22.4 %copy-start.17 = (f32[64]{0:T(128)S(1)}, f32[64]{0:T(128)}, u32[]{:S(2)}) copy-start(f32[64]{0:T(128)} %get-tuple-element.64) | copy-start | bytes 772
  228.1 22.4 %copy-start.18 = (f32[64]{0:T(128)S(1)}, f32[64]{0:T(128)}, u32[]{:S(2)}) copy-start(f32[64]{0:T(128)} %get-tuple-element.65) | copy-start | bytes 772
  228.2 22.4 %copy-start.19 = (f32[64]{0:T(128)S(1)}, f32[64]{0:T(128)}, u32[]{:S(2)}) copy-start(f32[64]{0:T(128)} %get-tuple-element.66) | copy-start | bytes 772
  228.2 22.4 %copy-start.20 = (f32[64]{0:T(128)S(1)}, f32[64]{0:T(128)}, u32[]{:S(2)}) copy-start(f32[64]{0:T(128)} %get-tuple-element.67) | copy-start | bytes 772
  228.2 22.4 %copy-start.21 = (f32[64]{0:T(128)S(1)}, f32[64]{0:T(128)}, u32[]{:S(2)}) copy-start(f32[64]{0:T(128)} %get-tuple-element.68) | copy-start | bytes 772
  228.2 22.4 %copy-start.22 = (f32[64]{0:T(128)S(1)}, f32[64]{0:T(128)}, u32[]{:S(2)}) copy-start(f32[64]{0:T(128)} %get-tuple-element.69) | copy-start | bytes 772
  228.2 22.4 %copy-start.23 = (f32[64]{0:T(128)S(1)}, f32[64]{0:T(128)}, u32[]{:S(2)}) copy-start(f32[64]{0:T(128)} %get-tuple-element.70) | copy-start | bytes 772
  228.2 22.4 %copy-start.24 = (f32[64]{0:T(128)S(1)}, f32[64]{0:T(128)}, u32[]{:S(2)}) copy-start(f32[64]{0:T(128)} %get-tuple-element.40) | copy-start | bytes 772
  228.2 22.4 %copy-start.25 = (f32[64]{0:T(128)S(1)}, f32[64]{0:T(128)}, u32[]{:S(2)}) copy-start(f32[64]{0:T(128)} %get-tuple-element.41) | copy-start | bytes 772
  228.2 22.4 %copy-start.26 = (f32[64]{0:T(128)S(1)}, f32[64]{0:T(128)}, u32[]{:S(2)}) copy-start(f32[64]{0:T(128)} %get-tuple-element.42) | copy-start | bytes 772
  228.2 22.4 %copy-start.27 = (f32[64]{0:T(128)S(1)}, f32[64]{0:T(128)}, u32[]{:S(2)}) copy-start(f32[64]{0:T(128)} %get-tuple-element.43) | copy-start | bytes 772
  228.3 22.4 %copy-start.28 = (f32[64]{0:T(128)S(1)}, f32[64]{0:T(128)}, u32[]{:S(2)}) copy-start(f32[64]{0:T(128)} %get-tuple-element.44) | copy-start | bytes 772
  230.5 28.5 %all-to-all-start.4 = ((bf16[32,2,2048]{2,1,0:T(2,128)(2,1)}), bf16[32,2,2048]{2,1,0:T(2,128)(2,1)S(1)}, u32[]{:S(2)}, u32[]{:S(2)}) async-start(bf16[32,2,2048]{2,1,0:T(2,128)(2,1)} %reshape.215), calls=%async_computation.4 | async-start | bytes 524288 | tf_op jit(solution)/shard_map/all_to_all | solution.py:39
  238.3 12.2 %collective-permute-start = (f32[30,64]{0,1:T(8,128)S(1)}, f32[30,64]{0,1:T(8,128)S(1)}, u32[]{:S(2)}, u32[]{:S(2)}) collective-permute-start(f32[30,64]{0,1:T(8,128)S(1)} %bitcast.167), channel_id=1, source_target_pairs={{16,0},{32,16},{48,32},{64,48},{80,64},{96,80},{112,96},{128,112},... | collective-permute-start | bytes 23048 | tf_op jit(solution)/shard_map/ppermute | solution.py:75
  (31 other events, 457.1 us)
Sparse Core Ops, SparseCore 0:
  57.3 62.0 all-gather.1
where the time goes:
time: 268 us; the launch traced here: 267 us
  waiting for transfers between devices  97.5 us (36%)
  blocking collectives  76 us (28%)
  starting transfers between devices  33.3 us (12%)
  local copies, waits for them, and re-layouts  21 us (8%)
  between operations  14.9 us (6%)
  matrix products  13.2 us (5%)
  other arithmetic  11.1 us (4%)
    all_gather x1, waiting for transfers between devices, in_one_piece(): lax.all_gather(both, axis, axis=dim, tiled=True)  62.2 us
    all_to_all x1, blocking collectives, side_by_side(): lax.all_to_all(both, axis, split_axis=split_dim, concat_axis=concat_dim,...  38.8 us
    all_gather x1, blocking collectives, shards(): lax.all_gather(out_proj, 'sp', axis=0, tiled=True)  37.3 us
    all_to_all x1, waiting for transfers between devices, shards(): lax.all_to_all(row_share.reshape(experts, capacity, slice_width), 'sp', s...  14.5 us
    all_to_all x2, starting transfers between devices, summed_on_arrival(): lax.all_to_all(blocks, axis, split_axis=0, concat_axis=0, tiled=True)  11.7 us
    all_to_all x2, starting transfers between devices, from_everyone(): return lax.all_to_all(copies, axis, split_axis=0, concat_axis=0, tiled=True)  10.4 us
    all_to_all x1, starting transfers between devices, shards(): lax.all_to_all(row_share.reshape(experts, capacity, slice_width), 'sp', s...  8.89 us
    ppermute x1, waiting for transfers between devices, passed_along(): lax.ppermute(value, axis, [(source, source + steps) for source in range(l...  8.54 us
  transfers between devices with their start and end apart: 7, of which 5 were waited for; matrix products, arithmetic and copies ran while one was open for 6% of the time, Pallas kernels for 0%

commit v1 on v0

v1 whole, which is shorter than its diff:
```python
import jax
import jax.numpy as jnp
from jax import lax
from jax.experimental import pallas as pl
from jax.experimental.pallas import tpu as pltpu
from jax.sharding import PartitionSpec as P

MESH = pl.DeviceIdType.MESH
F32 = jnp.float32
BF16 = jnp.bfloat16
ORDER = (0, 1, 15, 2, 14, 3, 13, 4, 12, 5, 11, 6, 10, 7, 9, 8)
PLACE = {r: i for i, r in enumerate(ORDER)}
G = 4
K = 8
HK = 4
QK = 2
FO = (0, 3, 1, 2)


def dot(a, b, ca, cb):
    return lax.dot_general(a, b, (((ca,), (cb,)), ((), ())), preferred_element_type=F32)


def iota(shape, dim):
    return lax.broadcasted_iota(jnp.int32, shape, dim)


def columns_of(row):
    return jnp.transpose(jnp.broadcast_to(row, (128, 128)))


def kernel(
    routes_ref, weight_ref, mi_ref, cot_ref, wg_ref, wu_ref, wd_ref, vv_ref, vg_ref, co_ref,
    mean_ref, rstd_ref, gain_ref, taps_ref, op_ref,
    gate_out, up_out, down_out, proj_out, stream_out, value_out, gating_out,
    S, X, W, GO, PB, T1, T2, Q, V, FN, RT, FS, DT, PT, OB, OPT, TT, TB, NM, FC, MX,
    GP, GI, GS, GR, SB, SR, CG, HB,
    w_sem, o_sem, sA, rA, sB, b1, b1f, b2, b2f, s1, r1, r2, s3, r3, sR, rR, sF, rF,
    sO, rO, sD, rD, sG, rG, sS, rS, sH, rH,
):
    sp, tp = lax.axis_index("sp"), lax.axis_index("tp")
    z, c = sp // 2, sp % 2
    y, x = tp // 4, tp % 4
    partner = z * 2 + 1 - c

    def J(h, fo, so):
        yy, xx = (so, fo) if h == 0 else (fo, so)
        return ((y + yy) % 4) * 4 + (x + xx) % 4

    def chip(d, core):
        return ((z + d) % 16) * 2 + core

    def send(src, dst, ssem, rsem, dev):
        pltpu.make_async_remote_copy(
            src_ref=src, dst_ref=dst, send_sem=ssem, recv_sem=rsem, device_id=dev, device_id_type=MESH
        ).start()

    def wait(ref, sem):
        pltpu.make_async_copy(ref, ref, sem).wait()

    barrier = pltpu.get_barrier_semaphore()
    for d in range(16):
        for core in range(2):
            if d == 0:
                continue
            pl.semaphore_signal(barrier, inc=1, device_id=(chip(d, core), tp), device_id_type=MESH)
    pl.semaphore_signal(barrier, inc=1, device_id=(partner, tp), device_id_type=MESH)
    for o in range(1, 16):
        pl.semaphore_signal(barrier, inc=1, device_id=(sp, J(0, o % 4, o // 4)), device_id_type=MESH)

    loads = [
        pltpu.make_async_copy(ref.at[0], W.at[176 * i : 176 * i + 176], w_sem.at[i])
        for i, ref in enumerate((wg_ref, wu_ref, wd_ref))
    ]
    for load in loads:
        load.start()

    r0, r1_ = routes_ref[0:1, :], routes_ref[1:2, :]
    ie = iota((32, 128), 0)
    m0 = jnp.where(ie == r0, 1.0, 0.0).astype(F32)
    m1 = jnp.where(ie == r1_, 1.0, 0.0).astype(F32)
    before = jnp.where(iota((128, 128), 0) < iota((128, 128), 1), 1.0, 0.0).astype(BF16)
    earlier = dot((m0 + m1).astype(BF16), before, 1, 0)
    t0 = r0.astype(F32) * 16.0 + jnp.sum(earlier * m0, axis=0, keepdims=True)
    t1 = r1_.astype(F32) * 16.0 + jnp.sum(earlier * m1, axis=0, keepdims=True)
    ir = iota((512, 128), 0).astype(F32)
    p0 = jnp.where(ir == t0, 1.0, 0.0)
    p1 = jnp.where(ir == t1, 1.0, 0.0)
    cot = cot_ref[...].astype(F32)
    c0 = (columns_of(weight_ref[0:1, :]) * cot).astype(BF16)
    c1 = (columns_of(weight_ref[1:2, :]) * cot).astype(BF16)
    rows = dot((p0 + p1).astype(BF16), mi_ref[...], 1, 0).astype(BF16)
    cots = (dot(p0.astype(BF16), c0, 1, 0) + dot(p1.astype(BF16), c1, 1, 0)).astype(BF16)
    S[:, 0] = rows.reshape(32, 16, 128)
    S[:, 1] = cots.reshape(32, 16, 128)

    pl.semaphore_wait(barrier, 46)

    send(S.at[partner], X.at[tp, c], sA, rA.at[0], (partner, tp))
    for r in ORDER[1:]:
        d = (16 - r) % 16
        q = PLACE[r] * 2
        for core in range(2):
            dest = chip(d, core)
            send(S.at[dest], X.at[tp, q + c], sA, rA.at[q // K], (dest, tp))
    X[tp, c] = S[sp]

    opt = jnp.transpose(jnp.pad(op_ref[...].astype(F32), ((0, 64), (0, 64))))
    lane = iota((32, 128), 1)
    OB[sp] = jnp.where(lane < 64, opt[0:32], pltpu.roll(opt[32:64], 64, 1)).astype(BF16)
    send(OB.at[sp], OB.at[sp], sO, rO, (partner, tp))
    for d in range(1, 16):
        for core in range(2):
            send(OB.at[sp], OB.at[sp], sO, rO, (chip(d, core), tp))

    k0, k1 = columns_of(t0), columns_of(t1)
    for n in range(4):
        il = (iota((128, 128), 1) + 128 * n).astype(F32)
        PT[:, 128 * n : 128 * n + 128] = jnp.where((k0 == il) | (k1 == il), 1.0, 0.0).astype(BF16)

    TT[...] = jnp.zeros_like(TT)
    TT[0:31, 0:64] = taps_ref[...].astype(F32)
    TT[31:32, 0:64] = gain_ref[...]
    tt = jnp.transpose(TT[...])
    gain = jnp.broadcast_to(tt[0:64, 31:32], (64, 128))
    for o in range(31):
        TB[o] = jnp.broadcast_to(tt[0:64, o : o + 1], (64, 128))
    normed = (co_ref[...].astype(F32) - mean_ref[...]) * rstd_ref[...]
    scaled = normed * gain
    sig = jax.nn.sigmoid(scaled)
    NM[...] = normed
    FC[...] = sig * (1.0 + scaled * (1.0 - sig)) * gain
    MX[...] = (scaled * sig).astype(BF16)
    SB[...] = jnp.zeros_like(SB)

    def q0(g, h):
        return g * K + h * HK

    def second(g, h, k):
        q = q0(g, h)
        piece = X.at[J(h, FO[k], 0), q : q + HK]
        send(piece, piece, sB, b2.at[g, h, k, 0], (sp, J(h, 0, 1)))
        send(piece, piece, sB, b2.at[g, h, k, 1], (sp, J(h, 0, 3)))

    def pass_on(g, h, k):
        q, fo = q0(g, h), FO[k]
        wait(X.at[J(h, fo, 3), q : q + HK], b2.at[g, h, k, 0])
        half = X.at[J(h, fo, 3), q : q + QK]
        send(half, half, sB, b2f.at[g, h, k, 0], (sp, J(h, 0, 1)))
        wait(X.at[J(h, fo, 1), q : q + HK], b2.at[g, h, k, 1])
        half = X.at[J(h, fo, 1), q + QK : q + HK]
        send(half, half, sB, b2f.at[g, h, k, 1], (sp, J(h, 0, 3)))

    def B0(g):
        first = 1 if g == 0 else 0
        wait(X.at[0, g * K + first : g * K + K], rA.at[g])
        for h in range(2):
            q = q0(g, h)
            piece = X.at[tp, q : q + HK]
            send(piece, piece, sB, b1.at[g, h, 0], (sp, J(h, 1, 0)))
            send(piece, piece, sB, b1.at[g, h, 1], (sp, J(h, 3, 0)))
            second(g, h, 0)

    def B1(g):
        for h in range(2):
            q = q0(g, h)
            own = J(h, 3, 0)
            wait(X.at[own, q : q + HK], b1.at[g, h, 0])
            half = X.at[own, q : q + QK]
            send(half, half, sB, b1f.at[g, h, 0], (sp, J(h, 1, 0)))
            own = J(h, 1, 0)
            wait(X.at[own, q : q + HK], b1.at[g, h, 1])
            half = X.at[own, q + QK : q + HK]
            send(half, half, sB, b1f.at[g, h, 1], (sp, J(h, 3, 0)))
            second(g, h, 1)
            second(g, h, 2)
        for h in range(2):
            pass_on(g, h, 0)

    def B2(g):
        for h in range(2):
            q = q0(g, h)
            own = J(h, 2, 0)
            wait(X.at[own, q : q + QK], b1f.at[g, h, 0])
            wait(X.at[own, q + QK : q + HK], b1f.at[g, h, 1])
            second(g, h, 3)
        for h in range(2):
            pass_on(g, h, 1)
            pass_on(g, h, 2)

    def B3(g):
        for h in range(2):
            pass_on(g, h, 3)

    def C(g):
        for h in range(2):
            q = q0(g, h)
            for k in range(4):
                own = J(h, FO[k], 2)
                wait(X.at[own, q : q + QK], b2f.at[g, h, k, 0])
                wait(X.at[own, q + QK : q + HK], b2f.at[g, h, k, 1])
        if g == 0:
            for load in loads:
                load.wait()
        part = []
        for a in range(2):
            part.append(
                jnp.concatenate(
                    [X[j, g * K : g * K + K, a].reshape(128, 128) for j in range(16)], axis=1
                )
            )
        both = dot(W[0:352], part[0], 1, 1)
        hg = dot(W[352:528], part[1], 1, 1)
        gate, up = both[0:176], both[176:352]
        gs = jax.nn.sigmoid(gate)
        act = gate * gs
        cols = slice(128 * g, 128 * g + 128)
        gd = (hg * up * gs * (1.0 + gate * (1.0 - gs))).astype(BF16)
        ud = (hg * act).astype(BF16)
        DT[0:176, cols] = gd
        DT[176:352, cols] = ud
        DT[352:528, cols] = (act * up).astype(BF16)
        partial = dot(DT[0:352, cols], W[0:352], 0, 0)
        for j in range(16):
            yy, xx = j // 4, j % 4
            block = partial[:, 128 * j : 128 * j + 128].astype(BF16)
            PB[g, 0, xx, yy] = block[0:64]
            PB[g, 1, yy, xx] = block[64:128]
        for h in range(2):
            f = (x, y)[h]
            far = (f + 2) % 4
            send(PB.at[g, h, far, 0:2], T1.at[g, h, 0], s1, r1.at[g, h, 0], (sp, J(h, 1, 0)))
            send(PB.at[g, h, far, 2:4], T1.at[g, h, 1], s1, r1.at[g, h, 1], (sp, J(h, 3, 0)))

    def R1(g):
        for h in range(2):
            f = (x, y)[h]
            nxt, prv = (f + 1) % 4, (f + 3) % 4
            wait(T1.at[g, h, 0], r1.at[g, h, 0])
            PB[g, h, nxt, 0:2] = (PB[g, h, nxt, 0:2].astype(F32) + T1[g, h, 0].astype(F32)).astype(BF16)
            send(PB.at[g, h, nxt], T2.at[g, h, 0], s1, r2.at[g, h, 0], (sp, J(h, 1, 0)))
            wait(T1.at[g, h, 1], r1.at[g, h, 1])
            PB[g, h, prv, 2:4] = (PB[g, h, prv, 2:4].astype(F32) + T1[g, h, 1].astype(F32)).astype(BF16)
            send(PB.at[g, h, prv], T2.at[g, h, 1], s1, r2.at[g, h, 1], (sp, J(h, 3, 0)))

    def R2(g):
        for h in range(2):
            f, s = ((x, y), (y, x))[h]
            wait(T2.at[g, h, 0], r2.at[g, h, 0])
            wait(T2.at[g, h, 1], r2.at[g, h, 1])
            Q[g, h] = (
                PB[g, h, f].astype(F32) + T2[g, h, 0].astype(F32) + T2[g, h, 1].astype(F32)
            ).astype(BF16)
            for d in range(1, 4):
                send(Q.at[g, h, (s + d) % 4], V.at[g, h, d - 1], s3, r3.at[g, h], (sp, J(h, 0, d)))

    def R3(g):
        for h in range(2):
            s = (y, x)[h]
            wait(V.at[g, h], r3.at[g, h])
            total = Q[g, h, s].astype(F32)
            for d in range(3):
                total = total + V[g, h, d].astype(F32)
            FN[g, h] = total.astype(BF16).reshape(HK, 16, 128)
            for k in range(HK):
                q = q0(g, h) + k
                r = ORDER[q // 2]
                if r == 0:
                    continue
                send(FN.at[g, h, k], RT.at[sp], sR, rR, (chip(r, q % 2), tp))
            if g == 0 and h == 0:
                send(FN.at[0, 0, 1 - c], RT.at[sp], sR, rR, (partner, tp))
                RT[sp] = FN[0, 0, c]

    def grads(lo, hi):
        def step(jp, carry):
            at = pl.ds(pl.multiple_of(jp * 256, 256), 256)
            rhs = jnp.concatenate(
                [X[2 * jp + i, :, 0].reshape(512, 128) for i in range(2)], axis=1
            )
            GO[0:352, at] = dot(DT[0:352], rhs, 1, 0).astype(BF16)
            rhs = jnp.concatenate(
                [X[2 * jp + i, :, 1].reshape(512, 128) for i in range(2)], axis=1
            )
            GO[352:528, at] = dot(DT[352:528], rhs, 1, 0).astype(BF16)
            return carry

        lax.fori_loop(lo, hi, step, 0)

    for t in range(G + 7):
        for fn, lag in ((B0, 0), (B1, 1), (B2, 2), (B3, 3), (R3, 7), (R2, 6), (R1, 5), (C, 4)):
            if 0 <= t - lag < G:
                fn(t - lag)
        if t >= G + 3:
            n = t - G - 3
            grads(2 * n, 2 * n + 2)

    stores = [
        pltpu.make_async_copy(GO.at[176 * i : 176 * i + 176], ref.at[0], o_sem.at[i])
        for i, ref in enumerate((gate_out, up_out, down_out))
    ]
    for store in stores:
        store.start()

    wait(OB.at[0:31], rO)
    for j in range(16):
        a, b = OB[2 * j].astype(F32), OB[2 * j + 1].astype(F32)
        OPT[0:32, 128 * j : 128 * j + 128] = jnp.where(lane < 64, a, pltpu.roll(b, 64, 1)).astype(BF16)
        OPT[32:64, 128 * j : 128 * j + 128] = jnp.where(lane < 64, pltpu.roll(a, 64, 1), b).astype(BF16)

    wait(RT.at[0:31], rR)
    mine = dot(PT[...], RT[...].reshape(512, 128), 1, 0)
    stream = (cot_ref[...].astype(F32) + mine).astype(BF16)
    FS[tp] = stream
    stream_out[...] = stream
    for o in range(1, 16):
        send(FS.at[tp], FS.at[tp], sF, rF, (sp, J(0, o % 4, o // 4)))
    wait(FS.at[0:15], rF)
    full = jnp.concatenate([FS[j] for j in range(16)], axis=1)

    gt = dot(MX[...], full, 1, 0)
    for k in range(16):
        top, bottom = gt[0:32, 128 * k : 128 * k + 128], gt[32:64, 128 * k : 128 * k + 128]
        GP[0, k] = jnp.where(lane < 64, top, pltpu.roll(bottom, 64, 1)).astype(BF16)
        GP[1, k] = jnp.where(lane < 64, pltpu.roll(top, 64, 1), bottom).astype(BF16)
    send(GP.at[1 - c], GI, sD, rD, (partner, tp))

    ng = dot(OPT[...], full, 1, 1) * FC[...]
    normed = NM[...]
    SB[0:1, :] = jnp.sum(ng, axis=0, keepdims=True)
    SB[1:2, :] = jnp.sum(ng * normed, axis=0, keepdims=True)
    for o in range(1, 16):
        send(SB, SR.at[tp], sS, rS, (sp, J(0, o % 4, o // 4)))
    SR[tp] = SB[...]

    wait(GI, rD)
    GS[...] = (GP[c].astype(F32) + GI[...].astype(F32)).astype(BF16)
    for d in range(1, 16):
        send(GS.at[(z + d) % 16], GR.at[z], sG, rG, (chip(d, c), tp))
    GR[z] = GS[z]

    wait(SR.at[0:15], rS)
    sums = jnp.sum(SR[...], axis=0) * (1.0 / 1024.0)
    cg = rstd_ref[...] * (ng - sums[0:1, :] - normed * sums[1:2, :])
    CG[...] = cg
    send(CG, HB, sH, rH, ((sp + 31) % 32, tp))
    wait(HB, rH)
    halo = jnp.where(sp == 31, 0.0, HB[...])
    lanes = iota((64, 128), 1)
    unit = TB[30] * cg
    for o in range(30):
        lead = 30 - o
        unit = unit + TB[o] * pltpu.roll(jnp.where(lanes >= lead, cg, halo), 128 - lead, 1)
    vs = jax.nn.sigmoid(vg_ref[...].astype(F32))
    value_out[...] = (unit * vs).astype(BF16)
    gating_out[...] = (unit * vv_ref[...].astype(F32) * vs * (1.0 - vs)).astype(BF16)

    wait(GR.at[0:15], rG)
    total = GR[0].astype(F32)
    for k in range(1, 16):
        total = total + GR[k].astype(F32)
    TT[0:32, :] = total
    TT[32:64, :] = pltpu.roll(total, 64, 1)
    proj_out[...] = jnp.transpose(TT[...])[0:64, 0:64]

    wait(S.at[0:31], sA)
    wait(OB.at[0:31], sO)
    wait(X.at[0:15], sB)
    wait(PB.at[0:3], s1)
    wait(Q.at[0:3], s3)
    wait(RT.at[0:31], sR)
    wait(FS.at[0:15], sF)
    wait(GI, sD)
    wait(GR.at[0:15], sG)
    wait(SR.at[0:15], sS)
    wait(HB, sH)
    for store in stores:
        store.wait()


def shards(
    moe_input, cotangent, routes, route_weight, w_gate, w_up, w_down, v_value, v_gate, conv_out,
    row_mean, row_rstd, ln_gain, taps, out_proj,
):
    vmem = pl.BlockSpec(memory_space=pltpu.VMEM)
    hbm = pl.BlockSpec(memory_space=pltpu.HBM)
    dma = pltpu.SemaphoreType.DMA
    v = pltpu.VMEM
    out = pl.pallas_call(
        kernel,
        out_shape=(
            jax.ShapeDtypeStruct((1, 176, 2048), BF16),
            jax.ShapeDtypeStruct((1, 176, 2048), BF16),
            jax.ShapeDtypeStruct((1, 176, 2048), BF16),
            jax.ShapeDtypeStruct((64, 64), F32),
            jax.ShapeDtypeStruct((128, 128), BF16),
            jax.ShapeDtypeStruct((64, 128), BF16),
            jax.ShapeDtypeStruct((64, 128), BF16),
        ),
        in_specs=[vmem] * 4 + [hbm] * 3 + [vmem] * 8,
        out_specs=(hbm, hbm, hbm, vmem, vmem, vmem, vmem),
        scratch_shapes=[
            v((32, 2, 16, 128), BF16),
            v((16, 32, 2, 16, 128), BF16),
            v((528, 2048), BF16),
            v((528, 2048), BF16),
            v((G, 2, 4, 4, 64, 128), BF16),
            v((G, 2, 2, 2, 64, 128), BF16),
            v((G, 2, 2, 4, 64, 128), BF16),
            v((G, 2, 4, 64, 128), BF16),
            v((G, 2, 3, 64, 128), BF16),
            v((G, 2, HK, 16, 128), BF16),
            v((32, 16, 128), BF16),
            v((16, 128, 128), BF16),
            v((528, 512), BF16),
            v((128, 512), BF16),
            v((32, 32, 128), BF16),
            v((64, 2048), BF16),
            v((128, 128), F32),
            v((31, 64, 128), F32),
            v((64, 128), F32),
            v((64, 128), F32),
            v((64, 128), BF16),
            v((2, 16, 32, 128), BF16),
            v((16, 32, 128), BF16),
            v((16, 32, 128), BF16),
            v((16, 32, 128), BF16),
            v((8, 128), F32),
            v((16, 8, 128), F32),
            v((64, 128), F32),
            v((64, 128), F32),
            dma((3,)), dma((3,)),
            dma(()), dma((G,)),
            dma(()), dma((G, 2, 2)), dma((G, 2, 2)), dma((G, 2, 4, 2)), dma((G, 2, 4, 2)),
            dma(()), dma((G, 2, 2)), dma((G, 2, 2)), dma(()), dma((G, 2)),
            dma(()), dma(()), dma(()), dma(()),
            dma(()), dma(()), dma(()), dma(()), dma(()), dma(()),
            dma(()), dma(()), dma(()), dma(()),
        ],
        compiler_params=pltpu.CompilerParams(
            collective_id=0, has_side_effects=True, vmem_limit_bytes=56 * 1024 * 1024
        ),
    )(
        routes.T, route_weight.T, moe_input, cotangent, w_gate, w_up, w_down, v_value.T, v_gate.T,
        conv_out.T, row_mean.reshape(1, 128), row_rstd.reshape(1, 128), ln_gain.reshape(1, 64), taps,
        out_proj,
    )
    gate_g, up_g, down_g, proj_g, stream, value_t, gating_t = out
    return gate_g, up_g, down_g, proj_g, stream, value_t.T, gating_t.T


def solution(mesh):
    return jax.shard_map(
        shards,
        mesh=mesh,
        in_specs=(
            P("sp", "tp"),
            P("sp", "tp"),
            P("sp", None),
            P("sp", None),
            P("sp", "tp", None),
            P("sp", "tp", None),
            P("sp", "tp", None),
            P("sp", "tp"),
            P("sp", "tp"),
            P("sp", "tp"),
            P("sp"),
            P("sp"),
            P("tp"),
            P(None, "tp"),
            P("sp", "tp"),
        ),
        out_specs=(
            P("sp", "tp", None),
            P("sp", "tp", None),
            P("sp", "tp", None),
            P("sp", "tp"),
            P("sp", "tp"),
            P("sp", "tp"),
            P("sp", "tp"),
        ),
        check_vma=False,
    )
```

time: 268 us -> 114 us (0.43)
  Pallas kernels: 0 us -> 106 us
  waiting for transfers between devices: 97.5 us -> 0 us
  blocking collectives: 76 us -> 0 us
  starting transfers between devices: 33.3 us -> 0 us
  between operations: 14.9 us -> 0.66 us
  local copies, waits for them, and re-layouts: 21 us -> 7.17 us
  matrix products: 13.2 us -> 0 us
  other arithmetic: 11.1 us -> 0 us
    pallas_call x0 -> x1, Pallas kernels: none -> 106 us  [shards(): pl.pallas_call(kernel, out_shape=(jax.ShapeDtypeStruct((1, 176, 2048), BF...]
    all_gather x1 -> x0, waiting for transfers between devices: 62.2 us -> none  [in_one_piece(): lax.all_gather(both, axis, axis=dim, tiled=True)]
    all_to_all x1 -> x0, blocking collectives: 38.8 us -> none  [side_by_side(): lax.all_to_all(both, axis, split_axis=split_dim, concat_axis=concat_dim,...]
    all_gather x1 -> x0, blocking collectives: 37.3 us -> none  [shards(): lax.all_gather(out_proj, 'sp', axis=0, tiled=True)]
    all_to_all x5 -> x0, starting transfers between devices: 31 us -> none  [the longest x2 11.7 us: summed_on_arrival(): lax.all_to_all(blocks, axis, split_axis=0, concat_axis=0, tiled=True)]
    all_to_all x5 -> x0, waiting for transfers between devices: 26.7 us -> none  [the longest x1 14.5 us: shards(): lax.all_to_all(row_share.reshape(experts, capacity, slice_width), 'sp', s...]
    dot_general x10 -> x0, matrix products: 13.2 us -> none  [the longest x4 7.12 us: contract_rows(): lax.dot_general(left, right, (((0,), (0,)), ((), ())), preferred_element_...]
    ppermute x1 -> x0, waiting for transfers between devices: 8.54 us -> none  [passed_along(): lax.ppermute(value, axis, [(source, source + steps) for source in range(l...]
  transfers between devices with their start and end apart: 7 -> 0, of which waited for: 5 -> 0; matrix products, arithmetic and copies ran while one was open for 6% -> 0% of each run, Pallas kernels for 0% -> 0%
where the time goes in v1:
time: 114 us; the launch traced here: 113 us
  Pallas kernels  106 us (93%)
  local copies, waits for them, and re-layouts  7.17 us (6%)
    pallas_call x1, Pallas kernels, shards(): pl.pallas_call(kernel, out_shape=(jax.ShapeDtypeStruct((1, 176, 2048), BF...  106 us
    unnamed x19, local copies, waits for them, and re-layouts  7.17 us

profile of v1, /device:TPU:1, one launch (start us, length us, event | category | flops | bytes accessed | tf_op | source)
XLA Modules:
  0.0 113.4 jit_solution(5203987230205379648)
XLA Ops:
  0.6 105.6 %shard_map.198 = (bf16[1,176,2048]{2,1,0:T(8,128)(2,1)}, bf16[1,176,2048]{2,1,0:T(8,128)(2,1)}, bf16[1,176,2048]{2,1,0:T(8,128)(2,1)}, f32[64,64]{1,0:T(8,128)},...) custom-call(s32[2,128]{1,0:T(2,128)} %bitcast.15, f32[2,128]{1,0:T(2,128)} %bitcast.16, ...), custom_call_target="tpu_custom_call" | custom-call | tf_op jit(solution)/shard_map/pallas_call | solution.py:389
  106.2 0.0 copy-start.1
  106.2 2.1 %copy.29 = bf16[1,176,2048]{2,1,0:T(8,128)(2,1)} copy(bf16[1,176,2048]{2,1,0:T(8,128)(2,1)} %get-tuple-element.28) | data formatting | bytes 1441792
  108.3 0.0 copy-done.1
  108.3 0.0 copy-start
  108.3 0.9 copy.30
  109.2 0.5 copy-done
  109.7 0.0 copy-start.3
  109.7 0.9 copy.31
  110.6 0.0 copy-done.3
  110.6 0.0 copy-start.2
  110.6 0.6 copy.32
  111.2 0.2 copy-done.2
  111.3 0.0 copy-start.5
  111.3 0.6 copy.33
  111.9 0.1 copy-done.5
  112.1 0.0 copy-start.4
  112.1 0.6 copy.34
  112.7 0.1 copy-done.4
  112.8 0.6 copy.35
Async XLA Ops:
  106.2 2.1 %copy-start.1 = (bf16[1,176,2048]{2,1,0:T(8,128)(2,1)S(1)}, bf16[1,176,2048]{2,1,0:T(8,128)(2,1)}, u32[]{:S(2)}) copy-start(bf16[1,176,2048]{2,1,0:T(8,128)(2,1)} %get-tuple-element.29) | copy-start | bytes 2162692
  108.3 1.4 %copy-start = (bf16[1,176,2048]{2,1,0:T(8,128)(2,1)S(1)}, bf16[1,176,2048]{2,1,0:T(8,128)(2,1)}, u32[]{:S(2)}) copy-start(bf16[1,176,2048]{2,1,0:T(8,128)(2,1)} %get-tuple-element.30) | copy-start | bytes 2162692
  109.7 0.9 copy-start.3
  110.6 0.8 copy-start.2
  111.3 0.7 copy-start.5
  112.1 0.7 copy-start.4

commit v2 on v1

--- a/solution.py
+++ b/solution.py
@@ -5,15 +5,21 @@
 from jax.experimental.pallas import tpu as pltpu
 from jax.sharding import PartitionSpec as P
 
+PEERS = (1, 3, 4, 12, 5, 7, 13, 15, 2, 8, 6, 9, 11, 14, 10)
 MESH = pl.DeviceIdType.MESH
 F32 = jnp.float32
 BF16 = jnp.bfloat16
-ORDER = (0, 1, 15, 2, 14, 3, 13, 4, 12, 5, 11, 6, 10, 7, 9, 8)
+ORDER = (0, 1, 15, 2, 8, 7, 9, 6, 10, 5, 11, 4, 12, 3, 13, 14)
 PLACE = {r: i for i, r in enumerate(ORDER)}
 G = 4
-K = 8
-HK = 4
-QK = 2
+STRIDE = 1
+STEPS = (("B0", 0), ("B1", 2), ("B2", 4), ("B3", 6), ("R3", 14), ("R2", 12), ("R1", 10), ("C", 8))
+OUT_AT = 3
+K = 32 // G
+HK = K // 2
+QK = K // 4
+RG = 16 * K
+RH = 16 * HK
 FO = (0, 3, 1, 2)
 
 
@@ -32,10 +38,10 @@
 def kernel(
     routes_ref, weight_ref, mi_ref, cot_ref, wg_ref, wu_ref, wd_ref, vv_ref, vg_ref, co_ref,
     mean_ref, rstd_ref, gain_ref, taps_ref, op_ref,
-    gate_out, up_out, down_out, proj_out, stream_out, value_out, gating_out,
-    S, X, W, GO, PB, T1, T2, Q, V, FN, RT, FS, DT, PT, OB, OPT, TT, TB, NM, FC, MX,
+    GO, proj_out, stream_out, value_out, gating_out,
+    S, X, W, PB, T1, T2, Q, V, FN, RT, FS, DT, PT, OB, OPT, TT, TB, NM, FC, MX,
     GP, GI, GS, GR, SB, SR, CG, HB,
-    w_sem, o_sem, sA, rA, sB, b1, b1f, b2, b2f, s1, r1, r2, s3, r3, sR, rR, sF, rF,
+    w_sem, sA, rA, sB, b1, b1f, b2, b2f, s1, r1, r2, s3, r3, sR, rR, sF, rF,
     sO, rO, sD, rD, sG, rG, sS, rS, sH, rH,
 ):
     sp, tp = lax.axis_index("sp"), lax.axis_index("tp")
@@ -108,10 +114,12 @@
     opt = jnp.transpose(jnp.pad(op_ref[...].astype(F32), ((0, 64), (0, 64))))
     lane = iota((32, 128), 1)
     OB[sp] = jnp.where(lane < 64, opt[0:32], pltpu.roll(opt[32:64], 64, 1)).astype(BF16)
-    send(OB.at[sp], OB.at[sp], sO, rO, (partner, tp))
-    for d in range(1, 16):
-        for core in range(2):
-            send(OB.at[sp], OB.at[sp], sO, rO, (chip(d, core), tp))
+
+    def share_projection():
+        send(OB.at[sp], OB.at[sp], sO, rO, (partner, tp))
+        for d in range(1, 16):
+            for core in range(2):
+                send(OB.at[sp], OB.at[sp], sO, rO, (chip(d, core), tp))
 
     k0, k1 = columns_of(t0), columns_of(t1)
     for n in range(4):
@@ -206,7 +214,7 @@
         for a in range(2):
             part.append(
                 jnp.concatenate(
-                    [X[j, g * K : g * K + K, a].reshape(128, 128) for j in range(16)], axis=1
+                    [X[j, g * K : g * K + K, a].reshape(RG, 128) for j in range(16)], axis=1
                 )
             )
         both = dot(W[0:352], part[0], 1, 1)
@@ -214,7 +222,7 @@
         gate, up = both[0:176], both[176:352]
         gs = jax.nn.sigmoid(gate)
         act = gate * gs
-        cols = slice(128 * g, 128 * g + 128)
+        cols = slice(RG * g, RG * g + RG)
         gd = (hg * up * gs * (1.0 + gate * (1.0 - gs))).astype(BF16)
         ud = (hg * act).astype(BF16)
         DT[0:176, cols] = gd
@@ -224,8 +232,8 @@
         for j in range(16):
             yy, xx = j // 4, j % 4
             block = partial[:, 128 * j : 128 * j + 128].astype(BF16)
-            PB[g, 0, xx, yy] = block[0:64]
-            PB[g, 1, yy, xx] = block[64:128]
+            PB[g, 0, xx, yy] = block[0:RH]
+            PB[g, 1, yy, xx] = block[RH:RG]
         for h in range(2):
             f = (x, y)[h]
             far = (f + 2) % 4
@@ -287,45 +295,63 @@
 
         lax.fori_loop(lo, hi, step, 0)
 
-    for t in range(G + 7):
-        for fn, lag in ((B0, 0), (B1, 1), (B2, 2), (B3, 3), (R3, 7), (R2, 6), (R1, 5), (C, 4)):
-            if 0 <= t - lag < G:
-                fn(t - lag)
-        if t >= G + 3:
-            n = t - G - 3
-            grads(2 * n, 2 * n + 2)
-
-    stores = [
-        pltpu.make_async_copy(GO.at[176 * i : 176 * i + 176], ref.at[0], o_sem.at[i])
-        for i, ref in enumerate((gate_out, up_out, down_out))
-    ]
-    for store in stores:
-        store.start()
+    plan = {"B0": B0, "B1": B1, "B2": B2, "B3": B3, "C": C, "R1": R1, "R2": R2, "R3": R3}
+    left = 0
+    for t in range(STRIDE * (G - 1) + 1 + max(lag for _, lag in STEPS)):
+        for name, lag in STEPS:
+            g, off = (t - lag) // STRIDE, (t - lag) % STRIDE
+            if off == 0 and 0 <= g < G:
+                plan[name](g)
+        if t == OUT_AT:
+            share_projection()
+        if t >= STRIDE * (G - 1) + STEPS[-1][1] and left < 8:
+            grads(left, left + 2)
+            left += 2
 
     wait(OB.at[0:31], rO)
     for j in range(16):
         a, b = OB[2 * j].astype(F32), OB[2 * j + 1].astype(F32)
-        OPT[0:32, 128 * j : 128 * j + 128] = jnp.where(lane < 64, a, pltpu.roll(b, 64, 1)).astype(BF16)
-        OPT[32:64, 128 * j : 128 * j + 128] = jnp.where(lane < 64, pltpu.roll(a, 64, 1), b).astype(BF16)
+        OPT[j, 0:32] = jnp.where(lane < 64, a, pltpu.roll(b, 64, 1)).astype(BF16)
+        OPT[j, 32:64] = jnp.where(lane < 64, pltpu.roll(a, 64, 1), b).astype(BF16)
 
     wait(RT.at[0:31], rR)
     mine = dot(PT[...], RT[...].reshape(512, 128), 1, 0)
     stream = (cot_ref[...].astype(F32) + mine).astype(BF16)
     FS[tp] = stream
     stream_out[...] = stream
-    for o in range(1, 16):
-        send(FS.at[tp], FS.at[tp], sF, rF, (sp, J(0, o % 4, o // 4)))
-    wait(FS.at[0:15], rF)
-    full = jnp.concatenate([FS[j] for j in range(16)], axis=1)
-
-    gt = dot(MX[...], full, 1, 0)
-    for k in range(16):
-        top, bottom = gt[0:32, 128 * k : 128 * k + 128], gt[32:64, 128 * k : 128 * k + 128]
+    for o in PEERS:
+        send(FS.at[tp], FS.at[tp], sF, rF.at[o], (sp, J(0, o % 4, o // 4)))
+    acc = jnp.zeros((64, 128), F32)
+
+    def pair_sum(o):
+        k = J(0, -o % 4, -(o // 4) % 4)
+        wait(GI.at[k], rD.at[o])
+        GS[k] = (GP[c, k].astype(F32) + GI[k].astype(F32)).astype(BF16)
+
+        @pl.when(k == z)
+        def _():
+            GR[z] = GS[z]
+
+        @pl.when(k != z)
+        def _():
+            send(GS.at[k], GR.at[z], sG, rG, (2 * k + c, tp))
+
+    pieces = (0,) + PEERS
+    for n, o in enumerate(pieces):
+        k = J(0, -o % 4, -(o // 4) % 4)
+        if o:
+            wait(FS.at[k], rF.at[o])
+        piece = FS[k]
+        gt = dot(MX[...], piece, 1, 0)
+        top, bottom = gt[0:32], gt[32:64]
         GP[0, k] = jnp.where(lane < 64, top, pltpu.roll(bottom, 64, 1)).astype(BF16)
         GP[1, k] = jnp.where(lane < 64, pltpu.roll(top, 64, 1), bottom).astype(BF16)
-    send(GP.at[1 - c], GI, sD, rD, (partner, tp))
-
-    ng = dot(OPT[...], full, 1, 1) * FC[...]
+        send(GP.at[1 - c, k], GI.at[k], sD, rD.at[o], (partner, tp))
+        acc = acc + dot(OPT[k], piece, 1, 1)
+        if n >= 4:
+            pair_sum(pieces[n - 4])
+
+    ng = acc * FC[...]
     normed = NM[...]
     SB[0:1, :] = jnp.sum(ng, axis=0, keepdims=True)
     SB[1:2, :] = jnp.sum(ng * normed, axis=0, keepdims=True)
@@ -333,11 +359,8 @@
         send(SB, SR.at[tp], sS, rS, (sp, J(0, o % 4, o // 4)))
     SR[tp] = SB[...]
 
-    wait(GI, rD)
-    GS[...] = (GP[c].astype(F32) + GI[...].astype(F32)).astype(BF16)
-    for d in range(1, 16):
-        send(GS.at[(z + d) % 16], GR.at[z], sG, rG, (chip(d, c), tp))
-    GR[z] = GS[z]
+    for o in pieces[12:]:
+        pair_sum(o)
 
     wait(SR.at[0:15], rS)
     sums = jnp.sum(SR[...], axis=0) * (1.0 / 1024.0)
@@ -366,16 +389,27 @@
     wait(S.at[0:31], sA)
     wait(OB.at[0:31], sO)
     wait(X.at[0:15], sB)
-    wait(PB.at[0:3], s1)
-    wait(Q.at[0:3], s3)
+    wait(PB.at[:, :, 0:3], s1)
+    wait(Q.at[:, :, 0:3], s3)
     wait(RT.at[0:31], sR)
     wait(FS.at[0:15], sF)
     wait(GI, sD)
     wait(GR.at[0:15], sG)
     wait(SR.at[0:15], sS)
     wait(HB, sH)
-    for store in stores:
-        store.wait()
+
+
+def finish(
+    go, proj, stream, value, gating,
+    gate_out, up_out, down_out, proj_out, stream_out, value_out, gating_out, sems,
+):
+    pairs = [(go.at[176 * i : 176 * i + 176], r.at[0]) for i, r in enumerate((gate_out, up_out, down_out))]
+    pairs += [(proj, proj_out), (stream, stream_out), (value, value_out), (gating, gating_out)]
+    copies = [pltpu.make_async_copy(a, b, sems.at[i]) for i, (a, b) in enumerate(pairs)]
+    for copy in copies:
+        copy.start()
+    for copy in copies:
+        copy.wait()
 
 
 def shards(
@@ -389,33 +423,30 @@
     out = pl.pallas_call(
         kernel,
         out_shape=(
-            jax.ShapeDtypeStruct((1, 176, 2048), BF16),
-            jax.ShapeDtypeStruct((1, 176, 2048), BF16),
-            jax.ShapeDtypeStruct((1, 176, 2048), BF16),
-            jax.ShapeDtypeStruct((64, 64), F32),
-            jax.ShapeDtypeStruct((128, 128), BF16),
-            jax.ShapeDtypeStruct((64, 128), BF16),
-            jax.ShapeDtypeStruct((64, 128), BF16),
+            v((528, 2048), BF16),
+            v((64, 64), F32),
+            v((128, 128), BF16),
+            v((64, 128), BF16),
+            v((64, 128), BF16),
         ),
         in_specs=[vmem] * 4 + [hbm] * 3 + [vmem] * 8,
-        out_specs=(hbm, hbm, hbm, vmem, vmem, vmem, vmem),
+        out_specs=(vmem,) * 5,
         scratch_shapes=[
             v((32, 2, 16, 128), BF16),
             v((16, 32, 2, 16, 128), BF16),
             v((528, 2048), BF16),
-            v((528, 2048), BF16),
-            v((G, 2, 4, 4, 64, 128), BF16),
-            v((G, 2, 2, 2, 64, 128), BF16),
-            v((G, 2, 2, 4, 64, 128), BF16),
-            v((G, 2, 4, 64, 128), BF16),
-            v((G, 2, 3, 64, 128), BF16),
+            v((G, 2, 4, 4, RH, 128), BF16),
+            v((G, 2, 2, 2, RH, 128), BF16),
+            v((G, 2, 2, 4, RH, 128), BF16),
+            v((G, 2, 4, RH, 128), BF16),
+            v((G, 2, 3, RH, 128), BF16),
             v((G, 2, HK, 16, 128), BF16),
             v((32, 16, 128), BF16),
             v((16, 128, 128), BF16),
             v((528, 512), BF16),
             v((128, 512), BF16),
             v((32, 32, 128), BF16),
-            v((64, 2048), BF16),
+            v((16, 64, 128), BF16),
             v((128, 128), F32),
             v((31, 64, 128), F32),
             v((64, 128), F32),
@@ -429,12 +460,12 @@
             v((16, 8, 128), F32),
             v((64, 128), F32),
             v((64, 128), F32),
-            dma((3,)), dma((3,)),
+            dma((3,)),
             dma(()), dma((G,)),
             dma(()), dma((G, 2, 2)), dma((G, 2, 2)), dma((G, 2, 4, 2)), dma((G, 2, 4, 2)),
             dma(()), dma((G, 2, 2)), dma((G, 2, 2)), dma(()), dma((G, 2)),
-            dma(()), dma(()), dma(()), dma(()),
-            dma(()), dma(()), dma(()), dma(()), dma(()), dma(()),
+            dma(()), dma(()), dma(()), dma((16,)),
+            dma(()), dma(()), dma(()), dma((16,)), dma(()), dma(()),
             dma(()), dma(()), dma(()), dma(()),
         ],
         compiler_params=pltpu.CompilerParams(
@@ -445,6 +476,16 @@
         conv_out.T, row_mean.reshape(1, 128), row_rstd.reshape(1, 128), ln_gain.reshape(1, 64), taps,
         out_proj,
     )
+    shapes = ((1, 176, 2048),) * 3 + ((64, 64), (128, 128), (64, 128), (64, 128))
+    kinds = (BF16, BF16, BF16, F32, BF16, BF16, BF16)
+    out = pl.pallas_call(
+        finish,
+        out_shape=tuple(jax.ShapeDtypeStruct(a, b) for a, b in zip(shapes, kinds)),
+        in_specs=[vmem] * 5,
+        out_specs=(hbm,) * 7,
+        scratch_shapes=[dma((7,))],
+        compiler_params=pltpu.CompilerParams(vmem_limit_bytes=4 * 1024 * 1024),
+    )(*out)
     gate_g, up_g, down_g, proj_g, stream, value_t, gating_t = out
     return gate_g, up_g, down_g, proj_g, stream, value_t.T, gating_t.T
 

time: 114 us -> 99.5 us (0.87)
  Pallas kernels: 106 us -> 98.6 us
  local copies, waits for them, and re-layouts: 7.17 us -> 0 us
    unnamed x19 -> x0, local copies, waits for them, and re-layouts: 7.17 us -> none
    pallas_call x1 -> x2, Pallas kernels: 106 us -> 98.6 us  [the longest x1 97.2 us: shards(): pl.pallas_call(kernel, out_shape=(v((528, 2048), BF16), v((64, 64), F32),...]
where the time goes in v2:
time: 99.5 us; the launch traced here: 99.3 us
  Pallas kernels  98.6 us (99%)
    pallas_call x1, Pallas kernels, shards(): pl.pallas_call(kernel, out_shape=(v((528, 2048), BF16), v((64, 64), F32),...  97.2 us

profile of v2, /device:TPU:1, one launch (start us, length us, event | category | flops | bytes accessed | tf_op | source)
XLA Modules:
  0.0 99.3 jit_solution(6721952165734049592)
XLA Ops:
  0.6 97.2 %shard_map.198 = (bf16[528,2048]{1,0:T(8,128)(2,1)S(1)}, f32[64,64]{1,0:T(8,128)S(1)}, bf16[128,128]{1,0:T(8,128)(2,1)S(1)}, bf16[64,128]{1,0:T(8,128)(2,1)S(1)}, bf16[64,128]{1,0:T(8,128)(2,1)S(1)}) custom-call(s32[2,128]{1,0:T(2,128)} %bitcast.13, f32[2,128]{1,0:T(2,128)} %bitcast.14, bf16[128,128]{1,0:T(8,128)(2,1)} %mi_ref.1, bf16[128,128]{1,0:T(8,128)(2,1)} %cot_ref.1, ...), custom_call_target="tpu_custom_call" | custom-call | tf_op jit(solution)/shard_map/pallas_call | solution.py:423
  97.9 1.4 %shard_map.199 = (bf16[1,176,2048]{2,1,0:T(8,128)(2,1)}, bf16[1,176,2048]{2,1,0:T(8,128)(2,1)}, bf16[1,176,2048]{2,1,0:T(8,128)(2,1)}, f32[64,64]{1,0:T(8,128)},...) custom-call(bf16[528,2048]{1,0:T(8,128)(2,1)S(1)} %get-tuple-element.19.go, ...), custom_call_target="tpu_custom_call" | custom-call | tf_op jit(solution)/shard_map/pallas_call | solution.py:481

commit v3 on v2

--- a/solution.py
+++ b/solution.py
@@ -13,14 +13,13 @@
 PLACE = {r: i for i, r in enumerate(ORDER)}
 G = 4
 STRIDE = 1
-STEPS = (("B0", 0), ("B1", 2), ("B2", 4), ("B3", 6), ("R3", 14), ("R2", 12), ("R1", 10), ("C", 8))
+STEPS = (("R3", 14), ("R2", 12), ("R1", 10), ("B3", 6), ("B2", 4), ("B1", 2), ("B0", 0), ("C", 8))
 OUT_AT = 3
 K = 32 // G
 HK = K // 2
 QK = K // 4
 RG = 16 * K
 RH = 16 * HK
-FO = (0, 3, 1, 2)
 
 
 def dot(a, b, ca, cb):
@@ -102,18 +101,39 @@
 
     pl.semaphore_wait(barrier, 46)
 
-    send(S.at[partner], X.at[tp, c], sA, rA.at[0], (partner, tp))
+    send(S.at[partner], X.at[y, x, c], sA, rA.at[0], (partner, tp))
     for r in ORDER[1:]:
         d = (16 - r) % 16
         q = PLACE[r] * 2
         for core in range(2):
             dest = chip(d, core)
-            send(S.at[dest], X.at[tp, q + c], sA, rA.at[q // K], (dest, tp))
-    X[tp, c] = S[sp]
-
-    opt = jnp.transpose(jnp.pad(op_ref[...].astype(F32), ((0, 64), (0, 64))))
+            send(S.at[dest], X.at[y, x, q + c], sA, rA.at[q // K], (dest, tp))
+    X[y, x, c] = S[sp]
+
     lane = iota((32, 128), 1)
-    OB[sp] = jnp.where(lane < 64, opt[0:32], pltpu.roll(opt[32:64], 64, 1)).astype(BF16)
+
+    def prepare():
+        opt = jnp.transpose(jnp.pad(op_ref[...].astype(F32), ((0, 64), (0, 64))))
+        OB[sp] = jnp.where(lane < 64, opt[0:32], pltpu.roll(opt[32:64], 64, 1)).astype(BF16)
+        k0, k1 = columns_of(t0), columns_of(t1)
+        for n in range(4):
+            il = (iota((128, 128), 1) + 128 * n).astype(F32)
+            PT[:, 128 * n : 128 * n + 128] = jnp.where((k0 == il) | (k1 == il), 1.0, 0.0).astype(BF16)
+
+        TT[...] = jnp.zeros_like(TT)
+        TT[0:31, 0:64] = taps_ref[...].astype(F32)
+        TT[31:32, 0:64] = gain_ref[...]
+        tt = jnp.transpose(TT[...])
+        gain = jnp.broadcast_to(tt[0:64, 31:32], (64, 128))
+        for o in range(31):
+            TB[o] = jnp.broadcast_to(tt[0:64, o : o + 1], (64, 128))
+        normed = (co_ref[...].astype(F32) - mean_ref[...]) * rstd_ref[...]
+        scaled = normed * gain
+        sig = jax.nn.sigmoid(scaled)
+        NM[...] = normed
+        FC[...] = sig * (1.0 + scaled * (1.0 - sig)) * gain
+        MX[...] = (scaled * sig).astype(BF16)
+        SB[...] = jnp.zeros_like(SB)
 
     def share_projection():
         send(OB.at[sp], OB.at[sp], sO, rO, (partner, tp))
@@ -121,92 +141,56 @@
             for core in range(2):
                 send(OB.at[sp], OB.at[sp], sO, rO, (chip(d, core), tp))
 
-    k0, k1 = columns_of(t0), columns_of(t1)
-    for n in range(4):
-        il = (iota((128, 128), 1) + 128 * n).astype(F32)
-        PT[:, 128 * n : 128 * n + 128] = jnp.where((k0 == il) | (k1 == il), 1.0, 0.0).astype(BF16)
-
-    TT[...] = jnp.zeros_like(TT)
-    TT[0:31, 0:64] = taps_ref[...].astype(F32)
-    TT[31:32, 0:64] = gain_ref[...]
-    tt = jnp.transpose(TT[...])
-    gain = jnp.broadcast_to(tt[0:64, 31:32], (64, 128))
-    for o in range(31):
-        TB[o] = jnp.broadcast_to(tt[0:64, o : o + 1], (64, 128))
-    normed = (co_ref[...].astype(F32) - mean_ref[...]) * rstd_ref[...]
-    scaled = normed * gain
-    sig = jax.nn.sigmoid(scaled)
-    NM[...] = normed
-    FC[...] = sig * (1.0 + scaled * (1.0 - sig)) * gain
-    MX[...] = (scaled * sig).astype(BF16)
-    SB[...] = jnp.zeros_like(SB)
-
     def q0(g, h):
         return g * K + h * HK
 
-    def second(g, h, k):
-        q = q0(g, h)
-        piece = X.at[J(h, FO[k], 0), q : q + HK]
-        send(piece, piece, sB, b2.at[g, h, k, 0], (sp, J(h, 0, 1)))
-        send(piece, piece, sB, b2.at[g, h, k, 1], (sp, J(h, 0, 3)))
-
-    def pass_on(g, h, k):
-        q, fo = q0(g, h), FO[k]
-        wait(X.at[J(h, fo, 3), q : q + HK], b2.at[g, h, k, 0])
-        half = X.at[J(h, fo, 3), q : q + QK]
-        send(half, half, sB, b2f.at[g, h, k, 0], (sp, J(h, 0, 1)))
-        wait(X.at[J(h, fo, 1), q : q + HK], b2.at[g, h, k, 1])
-        half = X.at[J(h, fo, 1), q + QK : q + HK]
-        send(half, half, sB, b2f.at[g, h, k, 1], (sp, J(h, 0, 3)))
+    def one(h, fo, lo, hi):
+        yy, xx = (0, fo) if h == 0 else (fo, 0)
+        return X.at[(y + yy) % 4, (x + xx) % 4, lo:hi]
+
+    def line(h, so, lo, hi):
+        return X.at[(y + so) % 4, :, lo:hi] if h == 0 else X.at[:, (x + so) % 4, lo:hi]
+
+    def copy_to(ref, sem, dev):
+        send(ref, ref, sB, sem, (sp, dev))
 
     def B0(g):
         first = 1 if g == 0 else 0
-        wait(X.at[0, g * K + first : g * K + K], rA.at[g])
+        wait(X.at[0, 0, g * K + first : g * K + K], rA.at[g])
         for h in range(2):
             q = q0(g, h)
-            piece = X.at[tp, q : q + HK]
-            send(piece, piece, sB, b1.at[g, h, 0], (sp, J(h, 1, 0)))
-            send(piece, piece, sB, b1.at[g, h, 1], (sp, J(h, 3, 0)))
-            second(g, h, 0)
+            copy_to(one(h, 0, q, q + HK), b1.at[g, h, 0], J(h, 1, 0))
+            copy_to(one(h, 0, q, q + HK), b1.at[g, h, 1], J(h, 3, 0))
 
     def B1(g):
         for h in range(2):
             q = q0(g, h)
-            own = J(h, 3, 0)
-            wait(X.at[own, q : q + HK], b1.at[g, h, 0])
-            half = X.at[own, q : q + QK]
-            send(half, half, sB, b1f.at[g, h, 0], (sp, J(h, 1, 0)))
-            own = J(h, 1, 0)
-            wait(X.at[own, q : q + HK], b1.at[g, h, 1])
-            half = X.at[own, q + QK : q + HK]
-            send(half, half, sB, b1f.at[g, h, 1], (sp, J(h, 3, 0)))
-            second(g, h, 1)
-            second(g, h, 2)
-        for h in range(2):
-            pass_on(g, h, 0)
+            wait(one(h, 3, q, q + HK), b1.at[g, h, 0])
+            copy_to(one(h, 3, q, q + QK), b1f.at[g, h, 0], J(h, 1, 0))
+            wait(one(h, 1, q, q + HK), b1.at[g, h, 1])
+            copy_to(one(h, 1, q + QK, q + HK), b1f.at[g, h, 1], J(h, 3, 0))
 
     def B2(g):
         for h in range(2):
             q = q0(g, h)
-            own = J(h, 2, 0)
-            wait(X.at[own, q : q + QK], b1f.at[g, h, 0])
-            wait(X.at[own, q + QK : q + HK], b1f.at[g, h, 1])
-            second(g, h, 3)
-        for h in range(2):
-            pass_on(g, h, 1)
-            pass_on(g, h, 2)
+            wait(one(h, 2, q, q + QK), b1f.at[g, h, 0])
+            wait(one(h, 2, q + QK, q + HK), b1f.at[g, h, 1])
+            copy_to(line(h, 0, q, q + HK), b2.at[g, h, 0], J(h, 0, 1))
+            copy_to(line(h, 0, q, q + HK), b2.at[g, h, 1], J(h, 0, 3))
 
     def B3(g):
         for h in range(2):
-            pass_on(g, h, 3)
+            q = q0(g, h)
+            wait(line(h, 3, q, q + HK), b2.at[g, h, 0])
+            copy_to(line(h, 3, q, q + QK), b2f.at[g, h, 0], J(h, 0, 1))
+            wait(line(h, 1, q, q + HK), b2.at[g, h, 1])
+            copy_to(line(h, 1, q + QK, q + HK), b2f.at[g, h, 1], J(h, 0, 3))
 
     def C(g):
         for h in range(2):
             q = q0(g, h)
-            for k in range(4):
-                own = J(h, FO[k], 2)
-                wait(X.at[own, q : q + QK], b2f.at[g, h, k, 0])
-                wait(X.at[own, q + QK : q + HK], b2f.at[g, h, k, 1])
+            wait(line(h, 2, q, q + QK), b2f.at[g, h, 0])
+            wait(line(h, 2, q + QK, q + HK), b2f.at[g, h, 1])
         if g == 0:
             for load in loads:
                 load.wait()
@@ -214,7 +198,7 @@
         for a in range(2):
             part.append(
                 jnp.concatenate(
-                    [X[j, g * K : g * K + K, a].reshape(RG, 128) for j in range(16)], axis=1
+                    [X[j // 4, j % 4, g * K : g * K + K, a].reshape(RG, 128) for j in range(16)], axis=1
                 )
             )
         both = dot(W[0:352], part[0], 1, 1)
@@ -284,11 +268,11 @@
         def step(jp, carry):
             at = pl.ds(pl.multiple_of(jp * 256, 256), 256)
             rhs = jnp.concatenate(
-                [X[2 * jp + i, :, 0].reshape(512, 128) for i in range(2)], axis=1
+                [X[jp // 2, 2 * (jp % 2) + i, :, 0].reshape(512, 128) for i in range(2)], axis=1
             )
             GO[0:352, at] = dot(DT[0:352], rhs, 1, 0).astype(BF16)
             rhs = jnp.concatenate(
-                [X[2 * jp + i, :, 1].reshape(512, 128) for i in range(2)], axis=1
+                [X[jp // 2, 2 * (jp % 2) + i, :, 1].reshape(512, 128) for i in range(2)], axis=1
             )
             GO[352:528, at] = dot(DT[352:528], rhs, 1, 0).astype(BF16)
             return carry
@@ -296,17 +280,17 @@
         lax.fori_loop(lo, hi, step, 0)
 
     plan = {"B0": B0, "B1": B1, "B2": B2, "B3": B3, "C": C, "R1": R1, "R2": R2, "R3": R3}
-    left = 0
     for t in range(STRIDE * (G - 1) + 1 + max(lag for _, lag in STEPS)):
         for name, lag in STEPS:
             g, off = (t - lag) // STRIDE, (t - lag) % STRIDE
             if off == 0 and 0 <= g < G:
                 plan[name](g)
+        if t == 0:
+            prepare()
         if t == OUT_AT:
             share_projection()
-        if t >= STRIDE * (G - 1) + STEPS[-1][1] and left < 8:
-            grads(left, left + 2)
-            left += 2
+
+    grads(0, 8)
 
     wait(OB.at[0:31], rO)
     for j in range(16):
@@ -388,7 +372,7 @@
 
     wait(S.at[0:31], sA)
     wait(OB.at[0:31], sO)
-    wait(X.at[0:15], sB)
+    wait(X.at[:, :, 0:30], sB)
     wait(PB.at[:, :, 0:3], s1)
     wait(Q.at[:, :, 0:3], s3)
     wait(RT.at[0:31], sR)
@@ -433,7 +417,7 @@
         out_specs=(vmem,) * 5,
         scratch_shapes=[
             v((32, 2, 16, 128), BF16),
-            v((16, 32, 2, 16, 128), BF16),
+            v((4, 4, 32, 2, 16, 128), BF16),
             v((528, 2048), BF16),
             v((G, 2, 4, 4, RH, 128), BF16),
             v((G, 2, 2, 2, RH, 128), BF16),
@@ -462,7 +446,7 @@
             v((64, 128), F32),
             dma((3,)),
             dma(()), dma((G,)),
-            dma(()), dma((G, 2, 2)), dma((G, 2, 2)), dma((G, 2, 4, 2)), dma((G, 2, 4, 2)),
+            dma(()), dma((G, 2, 2)), dma((G, 2, 2)), dma((G, 2, 2)), dma((G, 2, 2)),
             dma(()), dma((G, 2, 2)), dma((G, 2, 2)), dma(()), dma((G, 2)),
             dma(()), dma(()), dma(()), dma((16,)),
             dma(()), dma(()), dma(()), dma((16,)), dma(()), dma(()),

time: 99.5 us -> 97.8 us (0.983)
  Pallas kernels: 98.6 us -> 96.9 us
    pallas_call x1, Pallas kernels: 97.2 us -> 95.5 us  [shards(): pl.pallas_call(kernel, out_shape=(v((528, 2048), BF16), v((64, 64), F32),...]
where the time goes in v3:
time: 97.8 us; the launch traced here: 97.6 us
  Pallas kernels  96.9 us (99%)
    pallas_call x1, Pallas kernels, shards(): pl.pallas_call(kernel, out_shape=(v((528, 2048), BF16), v((64, 64), F32),...  95.5 us

profile of v3, /device:TPU:1, one launch (start us, length us, event | category | flops | bytes accessed | tf_op | source)
XLA Modules:
  0.0 97.6 jit_solution(3907563953218066824)
XLA Ops:
  0.6 95.5 %shard_map.198 = (bf16[528,2048]{1,0:T(8,128)(2,1)S(1)}, f32[64,64]{1,0:T(8,128)S(1)}, bf16[128,128]{1,0:T(8,128)(2,1)S(1)}, bf16[64,128]{1,0:T(8,128)(2,1)S(1)}, bf16[64,128]{1,0:T(8,128)(2,1)S(1)}) custom-call(s32[2,128]{1,0:T(2,128)} %bitcast.13, f32[2,128]{1,0:T(2,128)} %bitcast.14, bf16[128,128]{1,0:T(8,128)(2,1)} %mi_ref.1, bf16[128,128]{1,0:T(8,128)(2,1)} %cot_ref.1, ...), custom_call_target="tpu_custom_call" | custom-call | tf_op jit(solution)/shard_map/pallas_call | solution.py:407
  96.2 1.4 %shard_map.199 = (bf16[1,176,2048]{2,1,0:T(8,128)(2,1)}, bf16[1,176,2048]{2,1,0:T(8,128)(2,1)}, bf16[1,176,2048]{2,1,0:T(8,128)(2,1)}, f32[64,64]{1,0:T(8,128)},...) custom-call(bf16[528,2048]{1,0:T(8,128)(2,1)S(1)} %get-tuple-element.19.go, ...), custom_call_target="tpu_custom_call" | custom-call | tf_op jit(solution)/shard_map/pallas_call | solution.py:465
